TPU v7x, 32 devices: a whole 2x2x4 slice. The times are simulated.
32 devices in a mesh: sp: 8 (over z, y), tp: 4 (over x, core).
Axes of the slice: x: 2, y: 2, z: 4, core: 2. Of those that a mesh axis runs over, the one named last changes fastest.
Arguments:
- residual: bfloat16 [4, 768, 2048], P('tp', 'sp'), may hold values from -3 to 3
- query_nope: bfloat16 [4, 768, 1024], P('tp', 'sp'), may hold values from -9 to 9
- query_rope: bfloat16 [4, 768, 512], P('tp', 'sp'), may hold values from -48 to 48
- latent: bfloat16 [4, 768, 128], P('tp', 'sp'), may hold values from -6 to 6
- rope_key: bfloat16 [4, 768, 32], P('tp', 'sp'), may hold values from -48 to 48
- latent_gain: float32 [128], replicated, may hold values from 0.1 to 1.9
- up_key: bfloat16 [128, 1024], replicated, may hold values from -1 to 1
- up_value: bfloat16 [128, 1024], replicated, may hold values from -0.5 to 0.5
- out_weight: bfloat16 [1024, 2048], replicated, may hold values from -0.375 to 0.375
- ffn_gain: float32 [2048], replicated, may hold values from 0.1 to 1.9
- routes: int32 [4, 768, 2], P(None, 'sp'), may hold values from 0 to 7, all different within a row; in each aligned block of 96 rows (0 to 95, 96 to 191, ..., all dimensions but the last counted through in order) at most 30 rows name the same one
- route_weight: float32 [4, 768, 2], P('tp', 'sp'), may hold values from 0.1 to 1
- gate_weight: bfloat16 [8, 2048, 1024], P('sp', None, 'tp'), may hold values from -1.5 to 1.5
- up_weight: bfloat16 [8, 2048, 1024], P('sp', None, 'tp'), may hold values from -1.5 to 1.5
- down_weight: bfloat16 [8, 1024, 2048], P('sp', 'tp'), may hold values from -0.046875 to 0.046875
Outputs:
- updated: bfloat16 [4, 768, 2048], P('tp', 'sp')
Inputs may be any that keep to these rules, and one draw needn't show every extreme that they name: `routes`: each row names 2 different experts. In each aligned block of 96 rows (one sequence's rows of one device) no expert is named by more than 30 rows, a bound that some block reaches.
All inputs are finite; a program needn't handle non-finite values.
Results may differ from a plain program's by a relative error of at most 0.017.
Values may be sent and summed in bfloat16 or wider, within the bound.
A program may use at most 64 MiB of HBM per device.

v0:
```python
import math
import jax
import jax.numpy as jnp
from jax import lax
from jax.sharding import PartitionSpec as P

HEADS = 16
NOPE = 64
ROPE = 32
VDIM = 64
LATENT = 128
TOPK = 2
EPS = 1e-06
ROPE_BASE = 10000.0
CLAMP = 7.0
ALPHA = 1.702
NEG_BIG = -1e30


def rotate(values, positions, width):
    half = width // 2
    inverse = ROPE_BASE ** (-jnp.arange(half, dtype=jnp.float32) * 2.0 / width)
    angle = positions.astype(jnp.float32)[:, None] * inverse[None, :]
    cosine = jnp.cos(angle)[:, None, :]
    sine = jnp.sin(angle)[:, None, :]
    first = values[..., :half]
    second = values[..., half:]
    return jnp.concatenate(
        [first * cosine - second * sine, first * sine + second * cosine], axis=-1
    )


def rms_scaled(values, gain):
    return values * lax.rsqrt(jnp.mean(values * values, axis=-1, keepdims=True) + EPS) * gain


def block_rows(rows):
    return math.gcd(rows, 512)


def expert_term(rows, gate_w, up_w, down_w):
    gate = jnp.minimum(jnp.dot(rows, gate_w, preferred_element_type=jnp.float32), CLAMP)
    lift = jnp.clip(jnp.dot(rows, up_w, preferred_element_type=jnp.float32), -CLAMP, CLAMP)
    active = (gate * jax.nn.sigmoid(ALPHA * gate) * (lift + 1.0)).astype(jnp.bfloat16)
    return jnp.dot(active, down_w, preferred_element_type=jnp.float32)


def assign(picks, slots, count):
    flat = picks.reshape(-1)
    hot = (flat[:, None] == jnp.arange(count, dtype=jnp.int32)[None, :]).astype(jnp.int32)
    ranks = jnp.sum((jnp.cumsum(hot, axis=0) - 1) * hot, axis=1)
    return flat * slots + ranks


def pack_rows(rows, target, slots, count):
    tokens = rows.shape[0]
    owner = jnp.arange(target.shape[0], dtype=jnp.int32) // (target.shape[0] // tokens)
    source = jnp.full((count * slots,), tokens, jnp.int32).at[target].set(owner)
    padded = jnp.concatenate([rows, jnp.zeros((1, rows.shape[1]), rows.dtype)], axis=0)
    return padded[source]


def local(
    residual,
    query_nope,
    query_rope,
    latent,
    rope_key,
    latent_gain,
    up_key,
    up_value,
    out_weight,
    ffn_gain,
    routes,
    route_weight,
    gate_weight,
    up_weight,
    down_weight,
):
    tokens = residual.shape[1]
    width = residual.shape[2]
    experts = lax.axis_size("sp")
    slots = min(tokens, max(2, 5 * tokens * TOPK // (4 * experts)))
    positions = lax.axis_index("sp") * tokens + jnp.arange(tokens, dtype=jnp.int32)
    factor = (NOPE + ROPE) ** (-0.5)
    normed = rms_scaled(latent[0].astype(jnp.float32), latent_gain).astype(jnp.bfloat16)
    key_turned = rotate(rope_key[0].astype(jnp.float32)[:, None, :], positions, ROPE)[
        :, 0, :
    ].astype(jnp.bfloat16)
    query_plain = query_nope[0].reshape(tokens, HEADS, NOPE)
    query_turned = rotate(
        query_rope[0].astype(jnp.float32).reshape(tokens, HEADS, ROPE), positions, ROPE
    ).astype(jnp.bfloat16)
    initial = (
        jnp.full((HEADS, tokens), NEG_BIG, jnp.float32),
        jnp.zeros((HEADS, tokens), jnp.float32),
        jnp.zeros((tokens, HEADS, VDIM), jnp.float32),
    )
    carry = initial
    piece = (
        lax.all_gather(normed, "sp", axis=0, tiled=True),
        lax.all_gather(key_turned, "sp", axis=0, tiled=True),
    )
    rows = piece[0].shape[0]
    span = block_rows(rows)
    latent_blocks = piece[0].reshape(rows // span, span, LATENT)
    turned_blocks = piece[1].reshape(rows // span, span, ROPE)

    def step(state, blocks):
        peak_old, total, summed = state
        keys = jnp.dot(blocks[0], up_key, preferred_element_type=jnp.float32).astype(jnp.bfloat16)
        keys = keys.reshape(span, HEADS, NOPE)
        values = jnp.dot(blocks[0], up_value, preferred_element_type=jnp.float32).astype(
            jnp.bfloat16
        )
        values = values.reshape(span, HEADS, VDIM)
        scores = (
            jnp.einsum("qhd,khd->hqk", query_plain, keys, preferred_element_type=jnp.float32)
            + jnp.einsum("qhd,kd->hqk", query_turned, blocks[1], preferred_element_type=jnp.float32)
        ) * factor
        peak = jnp.maximum(peak_old, jnp.max(scores, axis=-1))
        shrink = jnp.exp(peak_old - peak)
        weights = jnp.exp(scores - peak[:, :, None])
        total = total * shrink + jnp.sum(weights, axis=-1)
        mixed = jnp.einsum(
            "hqk,khd->qhd", weights.astype(jnp.bfloat16), values, preferred_element_type=jnp.float32
        )
        summed = summed * jnp.transpose(shrink)[:, :, None] + mixed
        return ((peak, total, summed), None)

    carry, _ = lax.scan(step, carry, (latent_blocks, turned_blocks))
    peak, total, summed = carry
    attended = (
        (summed / jnp.transpose(total)[:, :, None])
        .reshape(tokens, HEADS * VDIM)
        .astype(jnp.bfloat16)
    )
    projected = jnp.dot(attended, out_weight, preferred_element_type=jnp.float32)
    middle = (residual[0].astype(jnp.float32) + projected).astype(jnp.bfloat16)
    middle_wide = middle.astype(jnp.float32)
    normal_rows = rms_scaled(middle_wide, ffn_gain).astype(jnp.bfloat16)
    own_picks = lax.dynamic_index_in_dim(routes, lax.axis_index("tp"), 0, keepdims=False)
    own_target = assign(own_picks, slots, experts)
    outgoing = pack_rows(normal_rows, own_target, slots, experts).reshape(1, experts, slots, width)
    arrived = lax.all_to_all(outgoing, "sp", split_axis=1, concat_axis=1, tiled=True)
    terms = expert_term(
        lax.all_gather(arrived, "tp", axis=0, tiled=True).reshape(-1, width),
        gate_weight[0],
        up_weight[0],
        down_weight[0],
    )
    mine = lax.psum_scatter(terms.astype(jnp.bfloat16), "tp", scatter_dimension=0, tiled=True)
    returned = lax.all_to_all(
        mine.reshape(1, experts, slots, width), "sp", split_axis=1, concat_axis=1, tiled=True
    )
    picked = returned.reshape(experts * slots, width)[own_target].reshape(tokens, TOPK, width)
    combined = jnp.sum(picked.astype(jnp.float32) * route_weight[0][:, :, None], axis=1)
    return (middle_wide + combined).astype(jnp.bfloat16)[None]


def solution(mesh):
    in_specs = (
        P("tp", "sp", None),
        P("tp", "sp", None),
        P("tp", "sp", None),
        P("tp", "sp", None),
        P("tp", "sp", None),
        P(),
        P(),
        P(),
        P(),
        P(),
        P(None, "sp", None),
        P("tp", "sp", None),
        P("sp", None, "tp"),
        P("sp", None, "tp"),
        P("sp", "tp", None),
    )
    out_specs = P("tp", "sp", None)
    return jax.shard_map(local, mesh=mesh, in_specs=in_specs, out_specs=out_specs, check_vma=False)
```

profile of v0, /device:TPU:0, one launch (start us, length us, event | category | flops | bytes accessed | tf_op | source)
XLA Modules:
  0.0 285.2 jit_solution(8489566156841574619)
XLA Ops:
  9.3 32.8 %all-gather = bf16[768,1,32]{2,1,0:T(2,128)(2,1)S(1)} all-gather(bf16[96,1,32]{2,1,0:T(2,128)(2,1)S(1)} %copy.46), channel_id=2, replica_groups=mesh['sp'=8,'tp'=4] {'sp'}, dimensions={0}, use_global_device_ids=true | all-gather | bytes 55296 | tf_op jit(solution)/shard_map/all_gather | solution.py:102
  42.8 32.6 %all_gather.9 = bf16[768,128]{1,0:T(8,128)(2,1)} all-gather(bf16[96,128]{1,0:T(8,128)(2,1)S(1)} %fusion.39), channel_id=1, replica_groups=mesh['sp'=8,'tp'=4] {'sp'}, dimensions={0}, use_global_device_ids=true | all-gather | bytes 221184 | tf_op jit(solution)/shard_map/all_gather | solution.py:101
  75.5 25.8 %while.15 = (s32[]{:T(128)}, f32[16,96]{1,0:T(8,128)S(1)}, f32[16,96]{1,0:T(8,128)}, f32[96,16,64]{0,2,1:T(8,128)}, bf16[3,256,128]{2,1,0:T(8,128)(2,1)}, /*inde...) while((s32[]{:T(128)}, f32[16,96]{1,0:T(8,128)S(1)}, ...), condition=%wide.region_4.5_spmd.clone, body=%wide.region_1.4_spmd.clone.sunk | while | flops 263627776 | bytes 14435629 | solution.py:131
  80.4 2.3 fusion.97
  88.9 2.5 fusion.97
  97.5 2.5 fusion.97
  102.4 3.2 %multiply_reduce_fusion.1 = (f32[96]{0:T(128)S(1)}, f32[96,2048]{1,0:T(8,128)S(1)}) fusion(bf16[96,1024]{0,1:T(8,128)(2,1)S(1)} %bitcast.107, bf16[1024,2048]{1,0:T(8,128)(2,1)} %param.25, bf16[1,96,2048]{2,1,0:T(8,128)(2,1)} %param.17), kind=kOutput, calls=%fused_computation.49 | convolution fusion | flops 403832736 | bytes 5570944 | tf_op jit(solution)/shard_map/dot_general | solution.py:138
  109.4 2.3 gather_fusion
  111.7 1.5 reshape.223
  113.1 21.4 %all_to_all.10 = bf16[1,8,30,2048]{3,2,0,1:T(8,128)(2,1)S(1)} all-to-all(bf16[1,8,30,2048]{3,2,0,1:T(8,128)(2,1)S(1)} %bitcast.106), channel_id=1, replica_groups=mesh['sp'=8,'tp'=4] {'sp'}, dimensions={1} | all-to-all | bytes 1966080 | tf_op jit(solution)/shard_map/all_to_all | solution.py:145
  134.5 1.5 copy.53
  136.3 31.9 %all-gather.3.cloned.1.call-done = bf16[4,8,30,2048]{3,1,2,0:T(8,128)(2,1)} async-done(((bf16[1,8,30,2048]{3,1,2,0:T(8,128)(2,1)}), bf16[4,8,30,2048]{3,1,2,0:T(8,128)(2,1)}) %all-gather.3.cloned.1.call-update) | async-done | bytes 3932176 | tf_op jit(solution)/shard_map/all_gather | solution.py:147
  168.2 6.3 %copy.54 = bf16[4,8,30,2048]{3,2,1,0:T(8,128)(2,1)} copy(bf16[4,8,30,2048]{3,1,2,0:T(8,128)(2,1)} %all-gather.3.cloned.1.call-done) | data formatting | bytes 7864320 | tf_op jit(solution)/shard_map/all_gather | solution.py:147
  174.5 5.1 %reshape.224 = bf16[960,2048]{1,0:T(8,128)(2,1)} reshape(bf16[4,8,30,2048]{3,2,1,0:T(8,128)(2,1)} %copy.54) | data formatting | bytes 7864320 | tf_op jit(solution)/shard_map/reshape | solution.py:147
  179.6 4.4 %convolution_minimum_fusion = f32[960,256]{1,0:T(8,128)} fusion(bf16[960,2048]{1,0:T(8,128)(2,1)} %reshape.224, bf16[1,2048,256]{2,1,0:T(8,128)(2,1)S(1)} %copy-done.12), kind=kOutput, calls=%fused_computation.34 | convolution fusion | flops 1006878720 | bytes 5963776 | tf_op jit(solution)/shard_map/dot_general | solution.py:42
  184.0 8.7 %convolution_convert_fusion.2 = bf16[960,2048]{1,0:T(8,128)(2,1)} fusion(bf16[960,2048]{1,0:T(8,128)(2,1)} %reshape.224, bf16[1,256,2048]{2,1,0:T(8,128)(2,1)S(1)} %copy-done, bf16[1,2048,256]{2,1,0:T(8,128)(2,1)} %param.30, f32[960,256]{1,0:T(8,128)} %convolution_minimum_fusion), kind=kOutput, calls=%fused_computation.28 | convolution fusion | flops 2017443840 | bytes 10944512 | tf_op jit(solution)/shard_map/dot_general | solution.py:45
  192.7 43.0 %reduce-scatter.2.cloned.1.call-done = bf16[240,2048]{1,0:T(8,128)(2,1)} async-done(((bf16[960,2048]{1,0:T(8,128)(2,1)}), bf16[240,2048]{1,0:T(8,128)(2,1)}) %reduce-scatter.2.cloned.1.call-update) | async-done | bytes 983056 | tf_op jit(solution)/shard_map/reduce_scatter | solution.py:152
  235.8 2.5 reshape.225
  238.2 5.5 %all-to-all-start.1 = ((bf16[1,8,30,2048]{3,2,0,1:T(8,128)(2,1)}), bf16[1,8,30,2048]{3,2,0,1:T(8,128)(2,1)}, u32[]{:S(2)}, u32[]{:S(2)}) async-start(bf16[1,8,30,2048]{3,2,0,1:T(8,128)(2,1)} %bitcast.19), calls=%async_computation.2 | async-start | bytes 2097152 | tf_op jit(solution)/shard_map/all_to_all | solution.py:153
  243.9 25.6 %all-to-all-done.1 = bf16[1,8,30,2048]{3,2,0,1:T(8,128)(2,1)} async-done(((bf16[1,8,30,2048]{3,2,0,1:T(8,128)(2,1)}), bf16[1,8,30,2048]{3,2,0,1:T(8,128)(2,1)}, u32[]{:S(2)}, u32[]{:S(2)}) %all-to-all-start.1) | async-done | bytes 983072 | tf_op jit(solution)/shard_map/all_to_all | solution.py:153
  269.5 1.5 reshape.226
  271.0 2.0 gather_fusion.1
  273.0 2.1 reshape.232
  275.2 2.3 multiply_reduce_fusion
  (129 shorter events, 27.6 us)
Async XLA Ops:
  6.5 177.4 %copy-start = (bf16[1,256,2048]{2,1,0:T(8,128)(2,1)S(1)}, bf16[1,256,2048]{2,1,0:T(8,128)(2,1)}, u32[]{:S(2)}) copy-start(bf16[1,256,2048]{2,1,0:T(8,128)(2,1)} %param.31) | copy-start | bytes 3145732
  6.5 35.9 %copy-start.7 = (bf16[1,96,1024]{2,1,0:T(8,128)(2,1)S(1)}, bf16[1,96,1024]{2,1,0:T(8,128)(2,1)}, u32[]{:S(2)}) copy-start(bf16[1,96,1024]{2,1,0:T(8,128)(2,1)} %param.18) | copy-start | bytes 589828
  6.5 36.0 %copy-start.8 = (bf16[1,96,128]{2,1,0:T(8,128)(2,1)S(1)}, bf16[1,96,128]{2,1,0:T(8,128)(2,1)}, u32[]{:S(2)}) copy-start(bf16[1,96,128]{2,1,0:T(8,128)(2,1)} %param.20) | copy-start | bytes 73732
  6.5 36.2 %copy-start.11 = (f32[128]{0:T(128)S(1)}, f32[128]{0:T(128)}, u32[]{:S(2)}) copy-start(f32[128]{0:T(128)} %param.22) | copy-start | bytes 1540
  6.5 161.7 %all-gather.3.cloned.1.call-start = ((), (), s32[]{:S(2)}) async-start(), calls=%async_computation.3 | async-start | bytes 4915200 | tf_op jit(solution)/shard_map/all_gather | solution.py:147
  75.5 2.0 copy-start.3
  75.6 2.5 copy-start.1
  82.7 0.7 copy-start.2
  82.7 0.7 copy-start.5
  82.7 1.3 copy-start.4
  84.0 1.9 copy-start.3
  84.0 2.5 copy-start.1
  91.4 0.7 copy-start.2
  91.4 0.7 copy-start.5
  91.4 1.3 copy-start.4
  92.7 1.9 copy-start.3
  92.7 2.5 copy-start.1
  100.0 0.7 copy-start.5
  100.0 1.3 copy-start.4
  102.4 6.8 %copy-start.9 = (f32[2048]{0:T(1024)S(1)}, f32[2048]{0:T(1024)}, u32[]{:S(2)}) copy-start(f32[2048]{0:T(1024)} %param.26) | copy-start | bytes 24580
  136.1 99.7 %reduce-scatter.2.cloned.1.call-start = ((), (), s32[]{:S(2)}) async-start(), calls=%async_computation.4 | async-start | bytes 4915200 | tf_op jit(solution)/shard_map/reduce_scatter | solution.py:152
  174.5 5.1 %copy-start.12 = (bf16[1,2048,256]{2,1,0:T(8,128)(2,1)S(1)}, bf16[1,2048,256]{2,1,0:T(8,128)(2,1)}, u32[]{:S(2)}) copy-start(bf16[1,2048,256]{2,1,0:T(8,128)(2,1)} %param.29) | copy-start | bytes 3145732
  192.7 51.0 %copy-start.10 = (f32[1,96,2]{1,2,0:T(2,128)S(1)}, f32[1,96,2]{1,2,0:T(2,128)}, u32[]{:S(2)}) copy-start(f32[1,96,2]{1,2,0:T(2,128)} %param.28) | copy-start | bytes 2308
  238.2 31.3 %all-to-all-start.1 = ((bf16[1,8,30,2048]{3,2,0,1:T(8,128)(2,1)}), bf16[1,8,30,2048]{3,2,0,1:T(8,128)(2,1)}, u32[]{:S(2)}, u32[]{:S(2)}) async-start(bf16[1,8,30,2048]{3,2,0,1:T(8,128)(2,1)} %bitcast.19), calls=%async_computation.2 | async-start | bytes 2097152 | tf_op jit(solution)/shard_map/all_to_all | solution.py:153
  (4 other events, 2.5 us)
Sparse Core Ops, SparseCore 0:
  136.2 31.9 all-gather.2
  192.8 42.8 reduce-scatter.1
where the time goes:
time: 286 us; the launch traced here: 285 us
  waiting for transfers between devices  101 us (35%)
  blocking collectives  86.8 us (30%)
  local copies, waits for them, and re-layouts  34.3 us (12%)
  matrix products  34.2 us (12%)
  between operations  13.7 us (5%)
  other arithmetic  9.43 us (3%)
  starting transfers between devices  5.77 us (2%)
    reduce_scatter x1, waiting for transfers between devices, local(): lax.psum_scatter(terms.astype(jnp.bfloat16), 'tp', scatter_dimension=0, t...  43 us
    all_gather x1, blocking collectives, local(): lax.all_gather(key_turned, 'sp', axis=0, tiled=True)  32.8 us
    all_gather x1, blocking collectives, local(): lax.all_gather(normed, 'sp', axis=0, tiled=True)  32.6 us
    all_gather x1, waiting for transfers between devices, local(): lax.all_gather(arrived, 'tp', axis=0, tiled=True).reshape(-1, width)  31.9 us
    all_to_all x1, waiting for transfers between devices, local(): lax.all_to_all(mine.reshape(1, experts, slots, width), 'sp', split_axis=1...  25.6 us
    all_to_all x1, blocking collectives, local(): lax.all_to_all(outgoing, 'sp', split_axis=1, concat_axis=1, tiled=True)  21.4 us
    dot_general x1, matrix products, expert_term(): return jnp.dot(active, down_w, preferred_element_type=jnp.float32)  8.72 us
    dot_general x3, matrix products, step(): jnp.einsum('hqk,khd->qhd', weights.astype(jnp.bfloat16), values, preferre...  7.3 us
  transfers between devices with their start and end apart: 3, of which 3 were waited for; matrix products, arithmetic and copies ran while one was open for 0% of the time, Pallas kernels for 0%

commit v1 on v0

--- a/solution.py
+++ b/solution.py
@@ -1,3 +1,4 @@
+import functools
 import math
 import jax
 import jax.numpy as jnp
@@ -15,6 +16,21 @@
 CLAMP = 7.0
 ALPHA = 1.702
 NEG_BIG = -1e30
+
+
+def convert_cubes(view, axis_tag):
+    return jnp.concatenate(
+        lax.all_to_all(
+            jnp.stack(jnp.split(view, lax.axis_size(axis_tag), 1), axis=0),
+            axis_tag,
+            split_axis=0,
+            concat_axis=0,
+        ),
+        1,
+    )
+
+
+find_stacks_all_now = functools.partial(convert_cubes, axis_tag="sp")
 
 
 def rotate(values, positions, width):
@@ -150,9 +166,7 @@
         down_weight[0],
     )
     mine = lax.psum_scatter(terms.astype(jnp.bfloat16), "tp", scatter_dimension=0, tiled=True)
-    returned = lax.all_to_all(
-        mine.reshape(1, experts, slots, width), "sp", split_axis=1, concat_axis=1, tiled=True
-    )
+    returned = find_stacks_all_now(mine.reshape(1, experts, slots, width))
     picked = returned.reshape(experts * slots, width)[own_target].reshape(tokens, TOPK, width)
     combined = jnp.sum(picked.astype(jnp.float32) * route_weight[0][:, :, None], axis=1)
     return (middle_wide + combined).astype(jnp.bfloat16)[None]

time: 286 us -> 290 us (1.014)
  local copies, waits for them, and re-layouts: 34.3 us -> 38.6 us
    unnamed x16 -> x23, local copies, waits for them, and re-layouts: 0.21 us -> 4.8 us
where the time goes in v1:
time: 290 us; the launch traced here: 289 us
  waiting for transfers between devices  101 us (35%)
  blocking collectives  86.8 us (30%)
  local copies, waits for them, and re-layouts  38.6 us (13%)
  matrix products  34.2 us (12%)
  between operations  13.7 us (5%)
  other arithmetic  9.43 us (3%)
  starting transfers between devices  5.77 us (2%)
    reduce_scatter x1, waiting for transfers between devices, local(): lax.psum_scatter(terms.astype(jnp.bfloat16), 'tp', scatter_dimension=0, t...  43.1 us
    all_gather x1, blocking collectives, local(): lax.all_gather(key_turned, 'sp', axis=0, tiled=True)  32.8 us
    all_gather x1, blocking collectives, local(): lax.all_gather(normed, 'sp', axis=0, tiled=True)  32.6 us
    all_gather x1, waiting for transfers between devices, local(): lax.all_gather(arrived, 'tp', axis=0, tiled=True).reshape(-1, width)  31.9 us
    all_to_all x1, waiting for transfers between devices, convert_cubes(): lax.all_to_all(jnp.stack(jnp.split(view, lax.axis_size(axis_tag), 1), axi...  25.6 us
    all_to_all x1, blocking collectives, local(): lax.all_to_all(outgoing, 'sp', split_axis=1, concat_axis=1, tiled=True)  21.4 us
    dot_general x1, matrix products, expert_term(): return jnp.dot(active, down_w, preferred_element_type=jnp.float32)  8.72 us
    dot_general x3, matrix products, step(): jnp.einsum('hqk,khd->qhd', weights.astype(jnp.bfloat16), values, preferre...  7.3 us
  transfers between devices with their start and end apart: 3, of which 3 were waited for; matrix products, arithmetic and copies ran while one was open for 0% of the time, Pallas kernels for 0%

profile of v1, /device:TPU:0, one launch (start us, length us, event | category | flops | bytes accessed | tf_op | source)
XLA Modules:
  0.0 289.4 jit_solution(17516614140264572818)
XLA Ops:
  9.3 32.8 %all-gather = bf16[768,1,32]{2,1,0:T(2,128)(2,1)S(1)} all-gather(bf16[96,1,32]{2,1,0:T(2,128)(2,1)S(1)} %copy.45), channel_id=2, replica_groups=mesh['sp'=8,'tp'=4] {'sp'}, dimensions={0}, use_global_device_ids=true | all-gather | bytes 55296 | tf_op jit(solution)/shard_map/all_gather | solution.py:118
  42.8 32.6 %all_gather.9 = bf16[768,128]{1,0:T(8,128)(2,1)} all-gather(bf16[96,128]{1,0:T(8,128)(2,1)S(1)} %fusion.47), channel_id=1, replica_groups=mesh['sp'=8,'tp'=4] {'sp'}, dimensions={0}, use_global_device_ids=true | all-gather | bytes 221184 | tf_op jit(solution)/shard_map/all_gather | solution.py:117
  75.5 25.8 %while.15 = (s32[]{:T(128)}, f32[16,96]{1,0:T(8,128)S(1)}, f32[16,96]{1,0:T(8,128)}, f32[96,16,64]{0,2,1:T(8,128)}, bf16[3,256,128]{2,1,0:T(8,128)(2,1)}, /*inde...) while((s32[]{:T(128)}, f32[16,96]{1,0:T(8,128)S(1)}, ...), condition=%wide.region_4.5_spmd.clone, body=%wide.region_1.4_spmd.clone.sunk | while | flops 263627776 | bytes 14435629 | solution.py:147
  80.4 2.3 fusion.105
  88.9 2.5 fusion.105
  97.5 2.5 fusion.105
  102.4 3.2 %multiply_reduce_fusion.1 = (f32[96]{0:T(128)S(1)}, f32[96,2048]{1,0:T(8,128)S(1)}) fusion(bf16[96,1024]{0,1:T(8,128)(2,1)S(1)} %bitcast.136, bf16[1024,2048]{1,0:T(8,128)(2,1)} %param.25, bf16[1,96,2048]{2,1,0:T(8,128)(2,1)} %param.17), kind=kOutput, calls=%fused_computation.49 | convolution fusion | flops 403832736 | bytes 5570944 | tf_op jit(solution)/shard_map/dot_general | solution.py:154
  109.4 2.3 gather_fusion
  111.7 1.5 reshape.220
  113.1 21.4 %all_to_all.10 = bf16[1,8,30,2048]{3,2,0,1:T(8,128)(2,1)S(1)} all-to-all(bf16[1,8,30,2048]{3,2,0,1:T(8,128)(2,1)S(1)} %bitcast.135), channel_id=1, replica_groups=mesh['sp'=8,'tp'=4] {'sp'}, dimensions={1} | all-to-all | bytes 1966080 | tf_op jit(solution)/shard_map/all_to_all | solution.py:161
  134.5 1.5 copy.52
  136.3 31.9 %all-gather.3.cloned.1.call-done = bf16[4,8,30,2048]{3,1,2,0:T(8,128)(2,1)} async-done(((bf16[1,8,30,2048]{3,1,2,0:T(8,128)(2,1)}), bf16[4,8,30,2048]{3,1,2,0:T(8,128)(2,1)}) %all-gather.3.cloned.1.call-update) | async-done | bytes 3932176 | tf_op jit(solution)/shard_map/all_gather | solution.py:163
  168.2 6.3 %copy.53 = bf16[4,8,30,2048]{3,2,1,0:T(8,128)(2,1)} copy(bf16[4,8,30,2048]{3,1,2,0:T(8,128)(2,1)} %all-gather.3.cloned.1.call-done) | data formatting | bytes 7864320 | tf_op jit(solution)/shard_map/all_gather | solution.py:163
  174.5 5.1 %reshape.221 = bf16[960,2048]{1,0:T(8,128)(2,1)} reshape(bf16[4,8,30,2048]{3,2,1,0:T(8,128)(2,1)} %copy.53) | data formatting | bytes 7864320 | tf_op jit(solution)/shard_map/reshape | solution.py:163
  179.6 4.4 %convolution_minimum_fusion = f32[960,256]{1,0:T(8,128)} fusion(bf16[960,2048]{1,0:T(8,128)(2,1)} %reshape.221, bf16[1,2048,256]{2,1,0:T(8,128)(2,1)S(1)} %copy-done.12), kind=kOutput, calls=%fused_computation.34 | convolution fusion | flops 1006878720 | bytes 5963776 | tf_op jit(solution)/shard_map/dot_general | solution.py:58
  184.0 8.7 %convolution_convert_fusion.2 = bf16[960,2048]{1,0:T(8,128)(2,1)} fusion(bf16[960,2048]{1,0:T(8,128)(2,1)} %reshape.221, bf16[1,256,2048]{2,1,0:T(8,128)(2,1)S(1)} %copy-done, bf16[1,2048,256]{2,1,0:T(8,128)(2,1)} %param.30, f32[960,256]{1,0:T(8,128)} %convolution_minimum_fusion), kind=kOutput, calls=%fused_computation.28 | convolution fusion | flops 2017443840 | bytes 10944512 | tf_op jit(solution)/shard_map/dot_general | solution.py:61
  192.7 43.1 %reduce-scatter.2.cloned.1.call-done = bf16[240,2048]{1,0:T(8,128)(2,1)} async-done(((bf16[960,2048]{1,0:T(8,128)(2,1)}), bf16[240,2048]{1,0:T(8,128)(2,1)}) %reduce-scatter.2.cloned.1.call-update) | async-done | bytes 983056 | tf_op jit(solution)/shard_map/reduce_scatter | solution.py:168
  235.8 1.5 reshape.222
  242.5 5.5 %all-to-all-start.1 = ((bf16[8,1,1,30,2048]{4,3,2,1,0:T(8,128)(2,1)}), bf16[8,1,1,30,2048]{4,3,2,1,0:T(8,128)(2,1)}, u32[]{:S(2)}, u32[]{:S(2)}) async-start(bf16[8,1,1,30,2048]{4,3,2,1,0:T(8,128)(2,1)} %fusion.37), calls=%async_computation.2 | async-start | bytes 2097152 | tf_op jit(solution)/shard_map/all_to_all | solution.py:23
  248.2 25.6 %all-to-all-done.1 = bf16[8,1,1,30,2048]{4,3,2,1,0:T(8,128)(2,1)} async-done(((bf16[8,1,1,30,2048]{4,3,2,1,0:T(8,128)(2,1)}), bf16[8,1,1,30,2048]{4,3,2,1,0:T(8,128)(2,1)}, u32[]{:S(2)}, u32[]{:S(2)}) %all-to-all-start.1) | async-done | bytes 983072 | tf_op jit(solution)/shard_map/all_to_all | solution.py:23
  273.8 1.5 reshape_reshape.3
  275.3 2.0 gather_fusion.1
  277.3 2.1 reshape.228
  279.5 2.3 multiply_reduce_fusion
  (137 shorter events, 32.9 us)
Async XLA Ops:
  6.5 177.4 %copy-start = (bf16[1,256,2048]{2,1,0:T(8,128)(2,1)S(1)}, bf16[1,256,2048]{2,1,0:T(8,128)(2,1)}, u32[]{:S(2)}) copy-start(bf16[1,256,2048]{2,1,0:T(8,128)(2,1)} %param.31) | copy-start | bytes 3145732
  6.5 35.9 %copy-start.7 = (bf16[1,96,1024]{2,1,0:T(8,128)(2,1)S(1)}, bf16[1,96,1024]{2,1,0:T(8,128)(2,1)}, u32[]{:S(2)}) copy-start(bf16[1,96,1024]{2,1,0:T(8,128)(2,1)} %param.18) | copy-start | bytes 589828
  6.5 36.0 %copy-start.8 = (bf16[1,96,128]{2,1,0:T(8,128)(2,1)S(1)}, bf16[1,96,128]{2,1,0:T(8,128)(2,1)}, u32[]{:S(2)}) copy-start(bf16[1,96,128]{2,1,0:T(8,128)(2,1)} %param.20) | copy-start | bytes 73732
  6.5 36.2 %copy-start.11 = (f32[128]{0:T(128)S(1)}, f32[128]{0:T(128)}, u32[]{:S(2)}) copy-start(f32[128]{0:T(128)} %param.22) | copy-start | bytes 1540
  6.5 161.7 %all-gather.3.cloned.1.call-start = ((), (), s32[]{:S(2)}) async-start(), calls=%async_computation.3 | async-start | bytes 4915200 | tf_op jit(solution)/shard_map/all_gather | solution.py:163
  75.5 2.0 copy-start.3
  75.6 2.5 copy-start.1
  82.7 0.7 copy-start.2
  82.7 0.7 copy-start.5
  82.7 1.3 copy-start.4
  84.0 1.9 copy-start.3
  84.0 2.5 copy-start.1
  91.4 0.7 copy-start.2
  91.4 0.7 copy-start.5
  91.4 1.3 copy-start.4
  92.7 1.9 copy-start.3
  92.7 2.5 copy-start.1
  100.0 0.7 copy-start.5
  100.0 1.3 copy-start.4
  102.4 6.8 %copy-start.9 = (f32[2048]{0:T(1024)S(1)}, f32[2048]{0:T(1024)}, u32[]{:S(2)}) copy-start(f32[2048]{0:T(1024)} %param.26) | copy-start | bytes 24580
  136.1 99.7 %reduce-scatter.2.cloned.1.call-start = ((), (), s32[]{:S(2)}) async-start(), calls=%async_computation.4 | async-start | bytes 4915200 | tf_op jit(solution)/shard_map/reduce_scatter | solution.py:168
  174.5 5.1 %copy-start.12 = (bf16[1,2048,256]{2,1,0:T(8,128)(2,1)S(1)}, bf16[1,2048,256]{2,1,0:T(8,128)(2,1)}, u32[]{:S(2)}) copy-start(bf16[1,2048,256]{2,1,0:T(8,128)(2,1)} %param.29) | copy-start | bytes 3145732
  239.9 8.2 %copy-start.10 = (f32[1,96,2]{1,2,0:T(2,128)S(1)}, f32[1,96,2]{1,2,0:T(2,128)}, u32[]{:S(2)}) copy-start(f32[1,96,2]{1,2,0:T(2,128)} %param.28) | copy-start | bytes 2308
  242.5 31.3 %all-to-all-start.1 = ((bf16[8,1,1,30,2048]{4,3,2,1,0:T(8,128)(2,1)}), bf16[8,1,1,30,2048]{4,3,2,1,0:T(8,128)(2,1)}, u32[]{:S(2)}, u32[]{:S(2)}) async-start(bf16[8,1,1,30,2048]{4,3,2,1,0:T(8,128)(2,1)} %fusion.37), calls=%async_computation.2 | async-start | bytes 2097152 | tf_op jit(solution)/shard_map/all_to_all | solution.py:23
  (4 other events, 2.5 us)
Sparse Core Ops, SparseCore 0:
  136.2 31.9 all-gather.2
  192.8 42.8 reduce-scatter.1
